TPU v7x, 512 devices: a whole 4x4x16 slice. The times are simulated.
512 devices in a mesh: sp: 16 (over z), dp: 32 (over y, x, core).
Axes of the slice: x: 4, y: 4, z: 16, core: 2. Of those that a mesh axis runs over, the one named last changes fastest.
Arguments:
- queries: bfloat16 [32, 3072, 16, 128], P('dp', 'sp'), may hold values from -6 to 6
- keys: bfloat16 [32, 3072, 16, 128], P('dp', 'sp'), may hold values from -6 to 6
- values: bfloat16 [32, 3072, 16, 128], P('dp', 'sp'), may hold values from -6 to 6
- mix_ratio: float32 [16], replicated, may hold values from 0.3 to 0.8
- out_gain: float32 [128], replicated, may hold values from 0.1 to 1.9
- out_weight: bfloat16 [2048, 2048], P(None, 'dp'), may hold values from -0.125 to 0.125
Outputs:
- layer_out: bfloat16 [32, 3072, 2048], P('dp', 'sp')
All inputs are finite; a program needn't handle non-finite values.
Results may differ from a plain program's by a relative error of at most 0.0098.
Values may be sent and summed in bfloat16 or wider, within the bound.
A program may use at most 64 MiB of HBM per device.

v0:
```python
import math

import jax
import jax.numpy as jnp
from jax import lax
from jax.sharding import PartitionSpec as P

theta_base = 500000.0
neg_large = -1e30
norm_eps = 1e-05


def in_one_piece(arrays, axis, split_dim, concat_dim, along):
    ends, at = ([], 0)
    for a in arrays[:-1]:
        at += a.shape[along]
        ends.append(at)
    both = jnp.concatenate(arrays, axis=along)
    return tuple(
        jnp.split(
            lax.all_to_all(both, axis, split_axis=split_dim, concat_axis=concat_dim, tiled=True),
            ends,
            axis=along,
        )
    )


def cut_along(array, dim, peers):
    before, after = (array.shape[:dim], array.shape[dim + 1 :])
    return jnp.moveaxis(array.reshape(*before, peers, -1, *after), dim, 0)


def piece_ends(length, count):
    turn = length // count
    if turn >= 8:
        turn -= turn % 8
    return [turn * k for k in range(1, count)]


def in_order(blocks, dim):
    dims = list(blocks.shape[1:])
    dims[dim] *= blocks.shape[0]
    return jnp.moveaxis(blocks, 0, dim).reshape(dims)


def exchange_in_pieces(array, axis, pieces, split_dim, concat_dim):
    blocks = cut_along(array, split_dim, lax.axis_size(axis))
    cut = max(range(1, max(2, blocks.ndim - 1)), key=lambda d: blocks.shape[d])
    outs = []
    for section in jnp.split(blocks, piece_ends(blocks.shape[cut], pieces), axis=cut):
        if section.size:
            outs.append(lax.all_to_all(section, axis, split_axis=0, concat_axis=0, tiled=True))
    return in_order(jnp.concatenate(outs, axis=cut), concat_dim)


def rotate_halves(field, positions):
    width = field.shape[-1] // 2
    half = width // 2
    freqs = theta_base ** (-jnp.arange(half, dtype=jnp.float32) * 2.0 / width)
    angle = positions.astype(jnp.float32)[:, None] * freqs[None, :]
    cosine = jnp.cos(angle)[:, None, :]
    sine = jnp.sin(angle)[:, None, :]
    parts = field.reshape(field.shape[0], 2, width)
    lower = parts[..., :half]
    upper = parts[..., half:]
    turned = jnp.concatenate(
        [lower * cosine - upper * sine, upper * cosine + lower * sine], axis=-1
    )
    return turned.reshape(field.shape)


def masked_softmax(scores, visible):
    kept = jnp.where(visible, scores, neg_large)
    highest = jnp.max(kept, axis=-1, keepdims=True)
    powers = jnp.exp(kept - highest)
    return powers / jnp.sum(powers, axis=-1, keepdims=True)


def head_attention(query_head, key_head, value_head, ratio, gain):
    length = query_head.shape[0]
    width = query_head.shape[1] // 2
    positions = jnp.arange(length, dtype=jnp.int32)
    rotated_queries = (
        rotate_halves(query_head.astype(jnp.float32), positions) * width ** (-0.5)
    ).astype(jnp.bfloat16)
    rotated_keys = rotate_halves(key_head.astype(jnp.float32), positions).astype(jnp.bfloat16)
    block = math.gcd(512, length)

    def one_block(start):
        query_rows = lax.dynamic_slice_in_dim(rotated_queries, start, block, 0)
        visible = (start + jnp.arange(block, dtype=jnp.int32))[:, None] >= positions[None, :]
        first = jnp.dot(
            query_rows[:, :width], rotated_keys[:, :width].T, preferred_element_type=jnp.float32
        )
        second = jnp.dot(
            query_rows[:, width:], rotated_keys[:, width:].T, preferred_element_type=jnp.float32
        )
        weights = (masked_softmax(first, visible) - ratio * masked_softmax(second, visible)).astype(
            jnp.bfloat16
        )
        mixed = jnp.dot(weights, value_head, preferred_element_type=jnp.float32)
        scale = lax.rsqrt(jnp.mean(mixed * mixed, axis=-1, keepdims=True) + norm_eps)
        return (mixed * scale * gain).astype(jnp.bfloat16)

    starts = jnp.arange(length // block, dtype=jnp.int32) * block
    return lax.map(one_block, starts).reshape(length, value_head.shape[1])


def on_device(queries, keys, values, mix_ratio, out_gain, out_weight):
    groups = lax.axis_size("sp")
    heads_here = queries.shape[2] // groups
    query_all, key_all, value_all = in_one_piece((queries, keys, values), "sp", 2, 1, 0)
    seqs = query_all.shape[0]
    length = query_all.shape[1]
    first_head = lax.axis_index("sp") * heads_here
    ratios = lax.dynamic_slice_in_dim(mix_ratio, first_head, heads_here, 0)
    item_ratios = jnp.tile(ratios, seqs)

    def by_item(field):
        return jnp.swapaxes(field, 1, 2).reshape(seqs * heads_here, length, field.shape[3])

    def one_head(head_items):
        query_head, key_head, value_head, ratio = head_items
        return head_attention(query_head, key_head, value_head, ratio, out_gain)

    heads = lax.map(
        one_head, (by_item(query_all), by_item(key_all), by_item(value_all), item_ratios)
    )
    attended = jnp.swapaxes(heads.reshape(seqs, heads_here, length, heads.shape[2]), 1, 2)
    returned = exchange_in_pieces(attended, "sp", 2, 1, 2)
    tokens_here = returned.shape[1]
    token_rows = returned.reshape(seqs * tokens_here, -1)
    result = jnp.dot(
        token_rows,
        lax.all_gather(out_weight, "dp", axis=1, tiled=True),
        preferred_element_type=jnp.float32,
    ).astype(jnp.bfloat16)
    return result.reshape(seqs, tokens_here, -1)


def solution(mesh):
    in_specs = (
        P("dp", "sp", None, None),
        P("dp", "sp", None, None),
        P("dp", "sp", None, None),
        P(),
        P(),
        P(None, "dp"),
    )
    out_specs = P("dp", "sp", None)
    return jax.shard_map(
        on_device, mesh=mesh, in_specs=in_specs, out_specs=out_specs, check_vma=False
    )
```

profile of v0, /device:TPU:6, one launch (start us, length us, event | category | flops | bytes accessed | tf_op | source)
XLA Modules:
  0.0 304.8 jit_solution(9597755954184421023)
XLA Ops:
  6.5 1.3 copy.15
  7.9 1.3 copy.16
  9.2 1.3 copy.17
  10.6 1.7 pad_maximum_fusion
  12.3 15.2 %all-to-all-start = ((bf16[3,192,16,128]{3,1,0,2:T(8,128)(2,1)}), bf16[3,192,16,128]{3,1,0,2:T(8,128)(2,1)S(1)}, u32[]{:S(2)}, u32[]{:S(2)}) async-start(bf16[3,192,16,128]{3,1,0,2:T(8,128)(2,1)} %pad_maximum_fusion), calls=%async_computation | async-start | bytes 4718592 | tf_op jit(solution)/shard_map/all_to_all | solution.py:21
  27.6 0.7 all-gather.2.cloned.1.call-update
  28.9 1.4 multiply_cosine_fusion
  30.3 103.8 %all-to-all-done = bf16[3,192,16,128]{3,1,0,2:T(8,128)(2,1)S(1)} async-done(((bf16[3,192,16,128]{3,1,0,2:T(8,128)(2,1)}), bf16[3,192,16,128]{3,1,0,2:T(8,128)(2,1)S(1)}, u32[]{:S(2)}, u32[]{:S(2)}) %all-to-all-start) | async-done | bytes 2359328 | tf_op jit(solution)/shard_map/all_to_all | solution.py:21
  134.1 2.1 fusion.19
  136.2 2.1 copy.18
  138.4 2.0 reshape.110
  140.3 2.1 copy.19
  142.5 2.1 reshape.111
  144.6 2.2 subtract_convert_fusion.2
  147.4 80.6 %while.18 = (s32[]{:T(128)}, bf16[6,512,128]{2,1,0:T(8,128)(2,1)}, s32[6]{0:T(128)S(1)}, bf16[3072,128]{0,1:T(8,128)(2,1)S(1)}, bf16[3072,128]{1,0:T(8,128)(2,1)...) while((s32[]{:T(128)}, bf16[6,512,128]{2,1,0:T(8,128)(2,1)}, ...), condition=%wide.region_6.7_spmd.clone, body=%wide.region_0.6_spmd.clone.sunk | while | flops 832371712 | bytes 44600544 | solution.py:106
  150.5 1.9 fusion.29
  152.3 1.7 fusion.28
  154.0 2.1 fusion.30
  156.1 3.8 %multiply_reduce_fusion.2 = (f32[512]{0:T(512)S(1)}, f32[512,128]{0,1:T(8,128)S(1)}) fusion(bf16[3072,128]{1,0:T(8,128)(2,1)S(1)} %copy-done, f32[512,3072]{1,0:T(8,128)S(1)} %get-tuple-element.202, f32[512,3072]{1,0:T(8,128)S(1)} %get-tuple-element.203, f32[512]{0:T(512)S(1)} %get-tuple-element.206, f32[512]{0:T(512)S(1)} %get-tuple-element.205, ...), kind=kOutput, calls=%fused_computation.13.clone.1 | convolution fusion | flops 413793792 | bytes 13641732 | tf_op jit(solution)/shard_map/while/body/eval_jaxpr/while/body/eval_jaxpr/dot_general | solution.py:101
  160.1 0.7 constant_dynamic-update-slice_fusion.2
  163.9 1.9 fusion.29
  165.8 1.7 fusion.28
  167.5 2.1 fusion.30
  169.6 3.8 %multiply_reduce_fusion.2 = (f32[512]{0:T(512)S(1)}, f32[512,128]{0,1:T(8,128)S(1)}) fusion(bf16[3072,128]{1,0:T(8,128)(2,1)S(1)} %copy-done, f32[512,3072]{1,0:T(8,128)S(1)} %get-tuple-element.202, f32[512,3072]{1,0:T(8,128)S(1)} %get-tuple-element.203, f32[512]{0:T(512)S(1)} %get-tuple-element.206, f32[512]{0:T(512)S(1)} %get-tuple-element.205, ...), kind=kOutput, calls=%fused_computation.13.clone.1 | convolution fusion | flops 413793792 | bytes 13641732 | tf_op jit(solution)/shard_map/while/body/eval_jaxpr/while/body/eval_jaxpr/dot_general | solution.py:101
  173.6 0.7 constant_dynamic-update-slice_fusion.2
  177.3 1.9 fusion.29
  179.2 1.7 fusion.28
  180.9 2.1 fusion.30
  183.0 3.8 %multiply_reduce_fusion.2 = (f32[512]{0:T(512)S(1)}, f32[512,128]{0,1:T(8,128)S(1)}) fusion(bf16[3072,128]{1,0:T(8,128)(2,1)S(1)} %copy-done, f32[512,3072]{1,0:T(8,128)S(1)} %get-tuple-element.202, f32[512,3072]{1,0:T(8,128)S(1)} %get-tuple-element.203, f32[512]{0:T(512)S(1)} %get-tuple-element.206, f32[512]{0:T(512)S(1)} %get-tuple-element.205, ...), kind=kOutput, calls=%fused_computation.13.clone.1 | convolution fusion | flops 413793792 | bytes 13641732 | tf_op jit(solution)/shard_map/while/body/eval_jaxpr/while/body/eval_jaxpr/dot_general | solution.py:101
  187.0 0.7 constant_dynamic-update-slice_fusion.2
  190.8 1.9 fusion.29
  192.6 1.7 fusion.28
  194.3 2.1 fusion.30
  196.4 3.8 %multiply_reduce_fusion.2 = (f32[512]{0:T(512)S(1)}, f32[512,128]{0,1:T(8,128)S(1)}) fusion(bf16[3072,128]{1,0:T(8,128)(2,1)S(1)} %copy-done, f32[512,3072]{1,0:T(8,128)S(1)} %get-tuple-element.202, f32[512,3072]{1,0:T(8,128)S(1)} %get-tuple-element.203, f32[512]{0:T(512)S(1)} %get-tuple-element.206, f32[512]{0:T(512)S(1)} %get-tuple-element.205, ...), kind=kOutput, calls=%fused_computation.13.clone.1 | convolution fusion | flops 413793792 | bytes 13641732 | tf_op jit(solution)/shard_map/while/body/eval_jaxpr/while/body/eval_jaxpr/dot_general | solution.py:101
  204.2 1.9 fusion.29
  206.1 1.7 fusion.28
  207.8 2.1 fusion.30
  209.9 3.8 %multiply_reduce_fusion.2 = (f32[512]{0:T(512)S(1)}, f32[512,128]{0,1:T(8,128)S(1)}) fusion(bf16[3072,128]{1,0:T(8,128)(2,1)S(1)} %copy-done, f32[512,3072]{1,0:T(8,128)S(1)} %get-tuple-element.202, f32[512,3072]{1,0:T(8,128)S(1)} %get-tuple-element.203, f32[512]{0:T(512)S(1)} %get-tuple-element.206, f32[512]{0:T(512)S(1)} %get-tuple-element.205, ...), kind=kOutput, calls=%fused_computation.13.clone.1 | convolution fusion | flops 413793792 | bytes 13641732 | tf_op jit(solution)/shard_map/while/body/eval_jaxpr/while/body/eval_jaxpr/dot_general | solution.py:101
  213.9 0.7 constant_dynamic-update-slice_fusion.2
  217.6 1.9 fusion.29
  219.5 1.7 fusion.28
  221.2 2.1 fusion.30
  223.3 3.8 %multiply_reduce_fusion.2 = (f32[512]{0:T(512)S(1)}, f32[512,128]{0,1:T(8,128)S(1)}) fusion(bf16[3072,128]{1,0:T(8,128)(2,1)S(1)} %copy-done, f32[512,3072]{1,0:T(8,128)S(1)} %get-tuple-element.202, f32[512,3072]{1,0:T(8,128)S(1)} %get-tuple-element.203, f32[512]{0:T(512)S(1)} %get-tuple-element.206, f32[512]{0:T(512)S(1)} %get-tuple-element.205, ...), kind=kOutput, calls=%fused_computation.13.clone.1 | convolution fusion | flops 413793792 | bytes 13641732 | tf_op jit(solution)/shard_map/while/body/eval_jaxpr/while/body/eval_jaxpr/dot_general | solution.py:101
  227.3 0.7 constant_dynamic-update-slice_fusion.2
  228.0 1.2 slice_bitcast_fusion.1
  229.1 31.4 %all_to_all.25 = bf16[16,1,96,1,128]{4,2,3,1,0:T(8,128)(2,1)S(1)} all-to-all(bf16[16,1,96,1,128]{4,2,3,1,0:T(8,128)(2,1)S(1)} %get-tuple-element.139), channel_id=1, replica_groups=mesh['sp'=16,'dp'=32] {'sp'}, dimensions={0} | all-to-all | bytes 786432 | tf_op jit(solution)/shard_map/all_to_all | solution.py:52
  260.5 29.6 %all_to_all.26 = bf16[16,1,96,1,128]{4,2,3,1,0:T(8,128)(2,1)S(1)} all-to-all(bf16[16,1,96,1,128]{4,2,3,1,0:T(8,128)(2,1)S(1)} %get-tuple-element.140), channel_id=1, replica_groups=mesh['sp'=16,'dp'=32] {'sp'}, dimensions={0} | all-to-all | bytes 786432 | tf_op jit(solution)/shard_map/all_to_all | solution.py:52
  290.8 7.2 %fusion.13 = bf16[1,192,2048]{2,1,0:T(8,128)(2,1)} fusion(bf16[2048,2048]{0,1:T(8,128)(2,1)} %all-gather.2.cloned.1.call-done, bf16[24,8,16,128]{3,2,1,0:T(8,128)(2,1)S(1)} %bitcast.46), kind=kOutput, calls=%fused_computation.22 | convolution fusion | flops 1611005952 | bytes 9961472 | tf_op jit(solution)/shard_map/dot_general | solution.py:133
  (59 shorter events, 11.1 us)
Async XLA Ops:
  7.9 20.4 %copy-start.2 = (f32[16]{0:T(128)S(1)}, f32[16]{0:T(128)}, u32[]{:S(2)}) copy-start(f32[16]{0:T(128)} %param.11) | copy-start | bytes 196
  12.3 121.8 %all-to-all-start = ((bf16[3,192,16,128]{3,1,0,2:T(8,128)(2,1)}), bf16[3,192,16,128]{3,1,0,2:T(8,128)(2,1)S(1)}, u32[]{:S(2)}, u32[]{:S(2)}) async-start(bf16[3,192,16,128]{3,1,0,2:T(8,128)(2,1)} %pad_maximum_fusion), calls=%async_computation | async-start | bytes 4718592 | tf_op jit(solution)/shard_map/all_to_all | solution.py:21
  27.5 263.3 %all-gather.2.cloned.1.call-start = ((), (), s32[]{:S(2)}) async-start(), calls=%async_computation.3 | async-start | bytes 8650752 | tf_op jit(solution)/shard_map/all_gather | solution.py:135
  144.6 2.8 copy-start.1
  154.0 2.1 copy-start
  167.5 2.1 copy-start
  180.9 2.1 copy-start
  194.3 2.1 copy-start
  207.8 2.1 copy-start
  221.2 2.1 copy-start
Sparse Core Ops, SparseCore 0:
  31.5 69.2 all-gather.1
where the time goes:
time: 305 us
  waiting for transfers between devices  105 us (34%)
  blocking collectives  61 us (20%)
  matrix products  51.1 us (17%)
  other arithmetic  24.6 us (8%)
  local copies, waits for them, and re-layouts  23.3 us (8%)
  starting transfers between devices  15.2 us (5%)
  between operations  13.5 us (4%)
  loops' own time  11.5 us (4%)
    all_to_all x1, waiting for transfers between devices, in_one_piece(): lax.all_to_all(both, axis, split_axis=split_dim, concat_axis=concat_dim,...  104 us
    all_to_all x2, blocking collectives, exchange_in_pieces(): lax.all_to_all(section, axis, split_axis=0, concat_axis=0, tiled=True)  61 us
    dot_general x6, matrix products, one_block(): mixed = jnp.dot(weights, value_head, preferred_element_type=jnp.float32)  22.5 us
    all_to_all x1, starting transfers between devices, in_one_piece(): lax.all_to_all(both, axis, split_axis=split_dim, concat_axis=concat_dim,...  15.2 us
    reduce_sum x6, other arithmetic, masked_softmax(): return powers / jnp.sum(powers, axis=-1, keepdims=True)  12.5 us
    another operation x1, loops' own time, head_attention(): return lax.map(one_block, starts).reshape(length, value_head.shape[1])  11.5 us
    dot_general x6, matrix products, one_block(): jnp.dot(query_rows[:, width:], rotated_keys[:, width:].T, preferred_eleme...  11.2 us
    dot_general x6, matrix products, one_block(): jnp.dot(query_rows[:, :width], rotated_keys[:, :width].T, preferred_eleme...  10.3 us
  transfers between devices with their start and end apart: 2, of which 1 were waited for; matrix products, arithmetic and copies ran while one was open for 28% of the time, Pallas kernels for 0%

commit v1 on v0

v1 whole, which is shorter than its diff:
```python
import functools

import jax
import jax.numpy as jnp
import numpy as np
from jax import lax
from jax.experimental import pallas as pl
from jax.experimental.pallas import tpu as pltpu
from jax.sharding import PartitionSpec as P

theta_base = 500000.0
neg_large = -1e30
norm_eps = 1e-05
MESH = pl.DeviceIdType.MESH
f32, bf16 = jnp.float32, jnp.bfloat16
CHUNK = 384


def peer_order(n):
    order = []
    for d in range(1, n // 2 + 1):
        order.append(d)
        if n - d != d:
            order.append(n - d)
    return order


def dot_nt(a, b):
    return lax.dot_general(a, b, (((1,), (1,)), ((), ())), preferred_element_type=f32)


def kernel(
    n, cores, rows, cols,
    mix_ref, q_hbm, k_hbm, v_hbm, gain_ref, freq_ref, w_hbm, out_ref,
    xin, win, xf, cos_s, sin_s, vs, ks, qs, vr, kr, qr, ob, ar, wt, qst, sc, mx, acc, oacc,
    in_sem, vss, kss, qss, oss, wss, wfs, vrs, krs, qrs, ars, wrs, wfr,
):
    me = lax.axis_index("sp")
    dp = lax.axis_index("dp")
    core = lax.rem(dp, 2)
    chip = lax.div(dp, 2)
    chips = cores // 2
    order = peer_order(n)

    loads = []
    for t, src in enumerate((v_hbm, k_hbm, q_hbm)):
        cp = pltpu.make_async_copy(src, xin.at[t], in_sem.at[t])
        cp.start()
        loads.append(cp)
    wload = pltpu.make_async_copy(w_hbm, win, in_sem.at[3])
    wload.start()

    barrier = pltpu.get_barrier_semaphore()
    for d in order:
        pl.semaphore_signal(barrier, inc=1, device_id={"sp": lax.rem(me + d, n)}, device_id_type=MESH)
    for d in range(1, chips):
        pl.semaphore_signal(
            barrier, inc=1, device_id={"dp": lax.rem(chip + d, chips) * 2 + core}, device_id_type=MESH
        )
    pl.semaphore_signal(barrier, inc=1, device_id={"dp": dp + 1 - 2 * core}, device_id_type=MESH)

    lane = lax.broadcasted_iota(jnp.int32, (rows, 128), 1)
    low = lax.rem(lane, 64) < 32
    pos = (lax.broadcasted_iota(jnp.int32, (rows, 128), 0) + me * rows).astype(f32)
    angle = pos * freq_ref[...]
    cos_s[...] = jnp.cos(angle)
    sine = jnp.sin(angle)
    sin_s[...] = jnp.where(low, -sine, sine)

    def widen(t):
        def step(j, _):
            r = pl.ds(pl.multiple_of(j * rows, rows), rows)
            xf[r, :] = xin[t, r, :].astype(f32)
            return 0

        lax.fori_loop(0, n, step, 0)

    def head_rows(h):
        return xf[pl.ds(h, rows, stride=n), :]

    def turned(h):
        x = head_rows(h)
        near = lax.broadcasted_iota(jnp.int32, (rows, 128), 1)
        other = jnp.where(lax.rem(near, 64) < 32, pltpu.roll(x, 96, 1), pltpu.roll(x, 32, 1))
        return x * cos_s[...] + other * sin_s[...]

    def start_all(src, dst, send, recv):
        for d in order:
            peer = lax.rem(me + d, n)
            pltpu.make_async_remote_copy(
                src_ref=src.at[peer],
                dst_ref=dst.at[pl.ds(pl.multiple_of(me * rows, rows), rows)],
                send_sem=send.at[d],
                recv_sem=recv.at[me],
                device_id={"sp": peer},
                device_id_type=MESH,
            ).start()

    mine = pl.ds(pl.multiple_of(me * rows, rows), rows)

    loads[0].wait()
    widen(0)

    def v_step(h, _):
        vs[h] = head_rows(h).astype(bf16)
        return 0

    lax.fori_loop(0, n, v_step, 0)
    loads[1].wait()
    widen(1)

    def k_step(h, _):
        ks[h] = turned(h).astype(bf16)
        return 0

    lax.fori_loop(0, n, k_step, 0)

    pl.semaphore_wait(barrier, n - 1 + chips - 1 + 1)
    start_all(vs, vr, vss, vrs)
    start_all(ks, kr, kss, krs)
    vr[mine, :] = vs[me]
    kr[mine, :] = ks[me]
    loads[2].wait()
    widen(2)

    def q_step(h, _):
        qs[h] = (turned(h) * 0.125).astype(bf16)
        return 0

    lax.fori_loop(0, n, q_step, 0)
    start_all(qs, qr, qss, qrs)
    qr[mine, :] = qs[me]

    wload.wait()
    eye = (
        lax.broadcasted_iota(jnp.int32, (cols, cols), 0) == lax.broadcasted_iota(jnp.int32, (cols, cols), 1)
    ).astype(bf16)

    def w_rows(owner):
        return pl.ds(pl.multiple_of(owner * cols, cols), cols)

    def wt_step(j, _):
        c = pl.ds(pl.multiple_of(j * 256, 256), 256)
        wt[w_rows(dp), c] = dot_nt(eye, win[c, :]).astype(bf16)
        return 0

    lax.fori_loop(0, win.shape[0] // 256, wt_step, 0)
    for d in range(1, chips):
        peer = lax.rem(chip + d, chips) * 2 + core
        pltpu.make_async_remote_copy(
            src_ref=wt.at[w_rows(dp)], dst_ref=wt.at[w_rows(dp)],
            send_sem=wss.at[d], recv_sem=wrs.at[chip],
            device_id={"dp": peer}, device_id_type=MESH,
        ).start()

    for d in order:
        src = lax.rem(me + n - d, n)
        pltpu.make_async_copy(vs.at[0], vr.at[mine], vrs.at[src]).wait()
        pltpu.make_async_copy(vs.at[0], kr.at[mine], krs.at[src]).wait()

    ratio = mix_ref[me]
    ones = jnp.ones((CHUNK, 128), bf16)

    def attend(i):
        q = qr[pl.ds(pl.multiple_of(i * rows, rows), rows), :]
        first = lax.broadcasted_iota(jnp.int32, (rows, 128), 1) < 64
        zero = jnp.zeros_like(q)
        qst[pl.ds(0, rows), :] = jnp.where(first, q, zero)
        qst[pl.ds(rows, rows), :] = jnp.where(first, zero, q)
        mx[...] = jnp.full_like(mx, neg_large)
        acc[...] = jnp.zeros_like(acc)
        count = lax.div((i + 1) * rows + CHUNK - 1, CHUNK)

        def chunk_rows(c):
            return pl.ds(pl.multiple_of(c * CHUNK, CHUNK), CHUNK)

        def put(c, s):
            sc[c] = s
            m = mx[...]
            for b in range(CHUNK // 128):
                m = jnp.maximum(m, s[:, b * 128 : (b + 1) * 128])
            mx[...] = m

        def score_step(c, _):
            put(c, dot_nt(qst[...], kr[chunk_rows(c), :]))
            return 0

        lax.fori_loop(0, count - 1, score_step, 0)
        last = count - 1
        s = dot_nt(qst[...], kr[chunk_rows(last), :])
        row = lax.broadcasted_iota(jnp.int32, (2 * rows, CHUNK), 0)
        row = jnp.where(row >= rows, row - rows, row) + i * rows
        col = lax.broadcasted_iota(jnp.int32, (2 * rows, CHUNK), 1) + last * CHUNK
        put(last, jnp.where(row >= col, s, neg_large))
        highest = jnp.max(mx[...], axis=1, keepdims=True)
        mx[...] = jnp.broadcast_to(highest, mx.shape)

        def weigh_step(c, _):
            m = mx[...]
            p = jnp.exp(sc[c] - jnp.concatenate([m] * (CHUNK // 128), axis=1)).astype(bf16)
            v = jnp.concatenate([vr[chunk_rows(c), :], ones], axis=1)
            acc[...] += jnp.dot(p, v, preferred_element_type=f32)
            return 0

        lax.fori_loop(0, count, weigh_step, 0)
        a = acc[...]
        mixed = a[:rows, :128] / a[:rows, 128:] - ratio * (a[rows:, :128] / a[rows:, 128:])
        scale = lax.rsqrt(jnp.mean(mixed * mixed, axis=1, keepdims=True) + norm_eps)
        return (mixed * scale * gain_ref[...]).astype(bf16)

    ar[me] = attend(me)

    def block_step(t, _):
        d = lax.div(t + 2, 2)
        i = lax.rem(jnp.where(lax.rem(t, 2) == 0, me + n - d, me + d), n)
        rows_i = pl.ds(pl.multiple_of(i * rows, rows), rows)
        pltpu.make_async_copy(vs.at[0], qr.at[rows_i], qrs.at[i]).wait()
        ob[i] = attend(i)
        pltpu.make_async_remote_copy(
            src_ref=ob.at[i], dst_ref=ar.at[me],
            send_sem=oss.at[i], recv_sem=ars.at[me],
            device_id={"sp": i}, device_id_type=MESH,
        ).start()
        return 0

    lax.fori_loop(0, n - 1, block_step, 0)

    partner = dp + 1 - 2 * core
    for d in range(0, chips):
        owner_chip = lax.rem(chip + chips - d, chips)
        owner = owner_chip * 2 + core
        if d:
            pltpu.make_async_copy(wt.at[w_rows(dp)], wt.at[w_rows(owner)], wrs.at[owner_chip]).wait()
        pltpu.make_async_remote_copy(
            src_ref=wt.at[w_rows(owner)], dst_ref=wt.at[w_rows(owner)],
            send_sem=wfs.at[owner_chip], recv_sem=wfr.at[owner_chip],
            device_id={"dp": partner}, device_id_type=MESH,
        ).start()
    for j in range(chips):
        other = j * 2 + 1 - core
        pltpu.make_async_copy(wt.at[w_rows(dp)], wt.at[w_rows(other)], wfr.at[j]).wait()

    def project(h, first):
        part = dot_nt(ar[h], wt[:, pl.ds(pl.multiple_of(h * 128, 128), 128)])
        if first:
            oacc[...] = part
        else:
            oacc[...] += part

    project(me, True)

    def project_step(t, _):
        d = lax.div(t + 2, 2)
        h = lax.rem(jnp.where(lax.rem(t, 2) == 0, me + n - d, me + d), n)
        pltpu.make_async_copy(vs.at[0], ar.at[h], ars.at[h]).wait()
        project(h, False)
        return 0

    lax.fori_loop(0, n - 1, project_step, 0)
    out_ref[...] = oacc[...].astype(bf16)

    for d in order:
        peer = lax.rem(me + d, n)
        pltpu.make_async_copy(vs.at[0], vr.at[mine], vss.at[d]).wait()
        pltpu.make_async_copy(vs.at[0], vr.at[mine], kss.at[d]).wait()
        pltpu.make_async_copy(vs.at[0], vr.at[mine], qss.at[d]).wait()
        pltpu.make_async_copy(vs.at[0], vr.at[mine], oss.at[peer]).wait()
    for d in range(1, chips):
        pltpu.make_async_copy(wt.at[w_rows(dp)], wt.at[w_rows(dp)], wss.at[d]).wait()
    for j in range(chips):
        pltpu.make_async_copy(wt.at[w_rows(dp)], wt.at[w_rows(dp)], wfs.at[j]).wait()


def on_device(queries, keys, values, mix_ratio, out_gain, out_weight):
    n = lax.axis_size("sp")
    cores = lax.axis_size("dp")
    _, rows, heads, width = queries.shape
    depth, cols = out_weight.shape
    total = n * rows
    half = width // 4
    freqs = theta_base ** (-np.arange(half, dtype=np.float32) * np.float32(2.0) / np.float32(width // 2))
    freqs = jnp.asarray(np.tile(freqs.astype(np.float32), 4)[None, :])
    hbm = pl.BlockSpec(memory_space=pltpu.MemorySpace.HBM)
    vmem = pl.BlockSpec(memory_space=pltpu.VMEM)
    dma = pltpu.SemaphoreType.DMA

    def flat(x):
        return x.reshape(rows * heads, width)

    out = pl.pallas_call(
        functools.partial(kernel, n, cores, rows, cols),
        out_shape=jax.ShapeDtypeStruct((rows, cores * cols), bf16),
        in_specs=[pl.BlockSpec(memory_space=pltpu.SMEM), hbm, hbm, hbm, vmem, vmem, hbm],
        out_specs=vmem,
        scratch_shapes=[
            pltpu.VMEM((3, rows * heads, width), bf16),
            pltpu.VMEM((depth, cols), bf16),
            pltpu.VMEM((rows * heads, width), f32),
            pltpu.VMEM((rows, width), f32),
            pltpu.VMEM((rows, width), f32),
            pltpu.VMEM((n, rows, width), bf16),
            pltpu.VMEM((n, rows, width), bf16),
            pltpu.VMEM((n, rows, width), bf16),
            pltpu.VMEM((total, width), bf16),
            pltpu.VMEM((total, width), bf16),
            pltpu.VMEM((total, width), bf16),
            pltpu.VMEM((n, rows, width), bf16),
            pltpu.VMEM((n, rows, width), bf16),
            pltpu.VMEM((cores * cols, depth), bf16),
            pltpu.VMEM((2 * rows, width), bf16),
            pltpu.VMEM((total // CHUNK, 2 * rows, CHUNK), f32),
            pltpu.VMEM((2 * rows, 128), f32),
            pltpu.VMEM((2 * rows, 256), f32),
            pltpu.VMEM((rows, cores * cols), f32),
            dma((4,)),
            dma((n,)), dma((n,)), dma((n,)), dma((n,)), dma((cores // 2,)), dma((cores // 2,)),
            dma((n,)), dma((n,)), dma((n,)), dma((n,)), dma((cores // 2,)), dma((cores // 2,)),
        ],
        compiler_params=pltpu.CompilerParams(
            collective_id=0, has_side_effects=True, vmem_limit_bytes=60 * 2**20
        ),
    )(mix_ratio, flat(queries), flat(keys), flat(values), out_gain.reshape(1, width), freqs, out_weight)
    return out[None]


def solution(mesh):
    tokens = P("dp", "sp", None, None)
    return jax.shard_map(
        on_device,
        mesh=mesh,
        in_specs=(tokens, tokens, tokens, P(), P(), P(None, "dp")),
        out_specs=P("dp", "sp", None),
        check_vma=False,
    )
```

time: 305 us -> 163 us (0.53)
  Pallas kernels: 0 us -> 158 us
  waiting for transfers between devices: 105 us -> 0 us
  blocking collectives: 61 us -> 0 us
  matrix products: 51.1 us -> 0 us
  other arithmetic: 24.6 us -> 0 us
  local copies, waits for them, and re-layouts: 23.3 us -> 4.04 us
  starting transfers between devices: 15.2 us -> 0 us
  between operations: 13.5 us -> 0.01 us
  loops' own time: 11.5 us -> 0 us
    pallas_call x0 -> x1, Pallas kernels: none -> 158 us  [on_device(): pl.pallas_call(functools.partial(kernel, n, cores, rows, cols), out_shape...]
    all_to_all x1 -> x0, waiting for transfers between devices: 104 us -> none  [in_one_piece(): lax.all_to_all(both, axis, split_axis=split_dim, concat_axis=concat_dim,...]
    all_to_all x2 -> x0, blocking collectives: 61 us -> none  [exchange_in_pieces(): lax.all_to_all(section, axis, split_axis=0, concat_axis=0, tiled=True)]
    dot_general x19 -> x0, matrix products: 51.1 us -> none  [the longest x6 22.5 us: one_block(): mixed = jnp.dot(weights, value_head, preferred_element_type=jnp.float32)]
    all_to_all x1 -> x0, starting transfers between devices: 15.2 us -> none  [in_one_piece(): lax.all_to_all(both, axis, split_axis=split_dim, concat_axis=concat_dim,...]
    reduce_sum x6 -> x0, other arithmetic: 12.5 us -> none  [masked_softmax(): return powers / jnp.sum(powers, axis=-1, keepdims=True)]
    another operation x1 -> x0, loops' own time: 11.5 us -> none  [head_attention(): return lax.map(one_block, starts).reshape(length, value_head.shape[1])]
    convert_element_type x4 -> x0, local copies, waits for them, and re-layouts: 8.32 us -> none  [the longest x2 4.2 us: head_attention(): key_head.astype(jnp.float32)]
  transfers between devices with their start and end apart: 2 -> 0, of which waited for: 1 -> 0; matrix products, arithmetic and copies ran while one was open for 28% -> 0% of each run, Pallas kernels for 0% -> 0%
where the time goes in v1:
time: 163 us; the launch traced here: 162 us
  Pallas kernels  158 us (97%)
  local copies, waits for them, and re-layouts  4.04 us (2%)
    pallas_call x1, Pallas kernels, on_device(): pl.pallas_call(functools.partial(kernel, n, cores, rows, cols), out_shape...  158 us
    unnamed x2, local copies, waits for them, and re-layouts  4.04 us

profile of v1, /device:TPU:6, one launch (start us, length us, event | category | flops | bytes accessed | tf_op | source)
XLA Modules:
  0.0 162.4 jit_solution(14837250598032948304)
XLA Ops:
  0.0 2.0 %copy.8.w_hbm = bf16[2048,64]{1,0:T(8,128)(2,1)} copy(bf16[2048,64]{0,1:T(8,128)(2,1)} %param.12) | data formatting | bytes 524288 | tf_op args[5]
  2.0 158.3 %shard_map.73 = bf16[192,2048]{1,0:T(8,128)(2,1)} custom-call(f32[16]{0:T(128)} %mix_ref.1, bf16[3072,128]{1,0:T(8,128)(2,1)} %bitcast.6, bf16[3072,128]{1,0:T(8,128)(2,1)} %bitcast.7, bf16[3072,128]{1,0:T(8,128)(2,1)} %bitcast.8, f32[1,128]{1,0:T(1,128)} %bitcast.9, f32[1,128]{1,0:T(1,128)} %constant.2.clone.freq_ref, bf16[2048,64]{1,0:T(8,128)(2,1)} %copy.8.w_hbm), custom_call_target="tpu_custom_call" | custom-call | tf_op jit(solution)/shard_map/pallas_call | solution.py:290
  160.3 2.1 %copy.10 = bf16[1,192,2048]{2,1,0:T(8,128)(2,1)} copy(bf16[1,192,2048]{2,1,0:T(8,128)(2,1)} %bitcast.5) | data formatting | bytes 1572864

commit v2 on v1

--- a/solution.py
+++ b/solution.py
@@ -32,7 +32,7 @@
 def kernel(
     n, cores, rows, cols,
     mix_ref, q_hbm, k_hbm, v_hbm, gain_ref, freq_ref, w_hbm, out_ref,
-    xin, win, xf, cos_s, sin_s, vs, ks, qs, vr, kr, qr, ob, ar, wt, qst, sc, mx, acc, oacc,
+    xin, xf, cos_s, sin_s, vs, ks, qs, vr, kr, qr, ob, ar, wt, qst, sc, mx, acc, oacc,
     in_sem, vss, kss, qss, oss, wss, wfs, vrs, krs, qrs, ars, wrs, wfr,
 ):
     me = lax.axis_index("sp")
@@ -47,7 +47,8 @@
         cp = pltpu.make_async_copy(src, xin.at[t], in_sem.at[t])
         cp.start()
         loads.append(cp)
-    wload = pltpu.make_async_copy(w_hbm, win, in_sem.at[3])
+    own_w = pl.ds(pl.multiple_of(dp * cols, cols), cols)
+    wload = pltpu.make_async_copy(w_hbm, wt.at[own_w], in_sem.at[3])
     wload.start()
 
     barrier = pltpu.get_barrier_semaphore()
@@ -132,19 +133,9 @@
     qr[mine, :] = qs[me]
 
     wload.wait()
-    eye = (
-        lax.broadcasted_iota(jnp.int32, (cols, cols), 0) == lax.broadcasted_iota(jnp.int32, (cols, cols), 1)
-    ).astype(bf16)
-
     def w_rows(owner):
         return pl.ds(pl.multiple_of(owner * cols, cols), cols)
 
-    def wt_step(j, _):
-        c = pl.ds(pl.multiple_of(j * 256, 256), 256)
-        wt[w_rows(dp), c] = dot_nt(eye, win[c, :]).astype(bf16)
-        return 0
-
-    lax.fori_loop(0, win.shape[0] // 256, wt_step, 0)
     for d in range(1, chips):
         peer = lax.rem(chip + d, chips) * 2 + core
         pltpu.make_async_remote_copy(
@@ -240,24 +231,23 @@
         other = j * 2 + 1 - core
         pltpu.make_async_copy(wt.at[w_rows(dp)], wt.at[w_rows(other)], wfr.at[j]).wait()
 
-    def project(h, first):
-        part = dot_nt(ar[h], wt[:, pl.ds(pl.multiple_of(h * 128, 128), 128)])
-        if first:
-            oacc[...] = part
-        else:
-            oacc[...] += part
-
-    project(me, True)
-
-    def project_step(t, _):
+    def project(h):
+        return dot_nt(ar[h], wt[:, pl.ds(pl.multiple_of(h * 128, 128), 128)])
+
+    def arrived(t):
         d = lax.div(t + 2, 2)
         h = lax.rem(jnp.where(lax.rem(t, 2) == 0, me + n - d, me + d), n)
         pltpu.make_async_copy(vs.at[0], ar.at[h], ars.at[h]).wait()
-        project(h, False)
-        return 0
-
-    lax.fori_loop(0, n - 1, project_step, 0)
-    out_ref[...] = oacc[...].astype(bf16)
+        return h
+
+    oacc[...] = project(me)
+
+    def project_step(t, _):
+        oacc[...] += project(arrived(t))
+        return 0
+
+    lax.fori_loop(0, n - 2, project_step, 0)
+    out_ref[...] = (oacc[...] + project(arrived(n - 2))).astype(bf16)
 
     for d in order:
         peer = lax.rem(me + d, n)
@@ -289,12 +279,11 @@
 
     out = pl.pallas_call(
         functools.partial(kernel, n, cores, rows, cols),
-        out_shape=jax.ShapeDtypeStruct((rows, cores * cols), bf16),
+        out_shape=pltpu.VMEM((rows, cores * cols), bf16),
         in_specs=[pl.BlockSpec(memory_space=pltpu.SMEM), hbm, hbm, hbm, vmem, vmem, hbm],
         out_specs=vmem,
         scratch_shapes=[
             pltpu.VMEM((3, rows * heads, width), bf16),
-            pltpu.VMEM((depth, cols), bf16),
             pltpu.VMEM((rows * heads, width), f32),
             pltpu.VMEM((rows, width), f32),
             pltpu.VMEM((rows, width), f32),
@@ -319,7 +308,7 @@
         compiler_params=pltpu.CompilerParams(
             collective_id=0, has_side_effects=True, vmem_limit_bytes=60 * 2**20
         ),
-    )(mix_ratio, flat(queries), flat(keys), flat(values), out_gain.reshape(1, width), freqs, out_weight)
+    )(mix_ratio, flat(queries), flat(keys), flat(values), out_gain.reshape(1, width), freqs, out_weight.T)
     return out[None]
 
 

time: 163 us -> 159 us (0.975)
  local copies, waits for them, and re-layouts: 4.04 us -> 0.88 us
    unnamed x2 -> x1, local copies, waits for them, and re-layouts: 4.04 us -> 0.88 us
where the time goes in v2:
time: 159 us; the launch traced here: 158 us
  Pallas kernels  158 us (99%)
    pallas_call x1, Pallas kernels, on_device(): pl.pallas_call(functools.partial(kernel, n, cores, rows, cols), out_shape...  158 us

profile of v2, /device:TPU:6, one launch (start us, length us, event | category | flops | bytes accessed | tf_op | source)
XLA Modules:
  0.0 158.5 jit_solution(12332859952068559607)
XLA Ops:
  0.0 157.6 %shard_map.73 = bf16[192,2048]{1,0:T(8,128)(2,1)S(1)} custom-call(f32[16]{0:T(128)} %mix_ref.1, bf16[3072,128]{1,0:T(8,128)(2,1)} %bitcast.7, bf16[3072,128]{1,0:T(8,128)(2,1)} %bitcast.8, bf16[3072,128]{1,0:T(8,128)(2,1)} %bitcast.9, f32[1,128]{1,0:T(1,128)} %bitcast.11, f32[1,128]{1,0:T(1,128)} %constant.2.clone.freq_ref, bf16[64,2048]{1,0:T(8,128)(2,1)} %bitcast.10), custom_call_target="tpu_custom_call" | custom-call | tf_op jit(solution)/shard_map/pallas_call | solution.py:280
  157.6 0.9 copy.9

commit v3 on v2

--- a/solution.py
+++ b/solution.py
@@ -13,6 +13,8 @@
 norm_eps = 1e-05
 MESH = pl.DeviceIdType.MESH
 f32, bf16 = jnp.float32, jnp.bfloat16
+EARLIER = (2, 4, 3, 2)
+LOW = len(EARLIER)
 CHUNK = 384
 
 
@@ -201,9 +203,11 @@
 
     ar[me] = attend(me)
 
-    def block_step(t, _):
+    def place(t):
         d = lax.div(t + 2, 2)
-        i = lax.rem(jnp.where(lax.rem(t, 2) == 0, me + n - d, me + d), n)
+        return lax.rem(jnp.where(lax.rem(t, 2) == 0, me + n - d, me + d), n)
+
+    def serve(i):
         rows_i = pl.ds(pl.multiple_of(i * rows, rows), rows)
         pltpu.make_async_copy(vs.at[0], qr.at[rows_i], qrs.at[i]).wait()
         ob[i] = attend(i)
@@ -212,6 +216,28 @@
             send_sem=oss.at[i], recv_sem=ars.at[me],
             device_id={"sp": i}, device_id_type=MESH,
         ).start()
+
+    def block_step(t, _):
+        def early_step(i, _):
+            r = lax.rem(me - i + n, n)
+            shift = EARLIER[0]
+            for q in range(1, LOW):
+                shift = jnp.where(i == q, EARLIER[q], shift)
+            turn = jnp.maximum(jnp.where(r <= n // 2, 2 * r - 2, 2 * (n - r) - 1) - shift, 0)
+
+            @pl.when((i != me) & (turn == t))
+            def _():
+                serve(i)
+
+            return 0
+
+        lax.fori_loop(0, LOW, early_step, 0)
+        i = place(t)
+
+        @pl.when(i >= LOW)
+        def _():
+            serve(i)
+
         return 0
 
     lax.fori_loop(0, n - 1, block_step, 0)
@@ -235,8 +261,7 @@
         return dot_nt(ar[h], wt[:, pl.ds(pl.multiple_of(h * 128, 128), 128)])
 
     def arrived(t):
-        d = lax.div(t + 2, 2)
-        h = lax.rem(jnp.where(lax.rem(t, 2) == 0, me + n - d, me + d), n)
+        h = place(t)
         pltpu.make_async_copy(vs.at[0], ar.at[h], ars.at[h]).wait()
         return h
 

time: 159 us -> 157 us (0.987)
  the two profiles are of different devices: /device:TPU:6 before, /device:TPU:32 now
where the time goes in v3:
time: 157 us
  Pallas kernels  156 us (99%)
    pallas_call x1, Pallas kernels, on_device(): pl.pallas_call(functools.partial(kernel, n, cores, rows, cols), out_shape...  156 us

profile of v3, /device:TPU:32, one launch (start us, length us, event | category | flops | bytes accessed | tf_op | source)
XLA Modules:
  0.0 157.1 jit_solution(4495375770868754735)
XLA Ops:
  0.0 156.3 %shard_map.73 = bf16[192,2048]{1,0:T(8,128)(2,1)S(1)} custom-call(f32[16]{0:T(128)} %mix_ref.1, bf16[3072,128]{1,0:T(8,128)(2,1)} %bitcast.7, bf16[3072,128]{1,0:T(8,128)(2,1)} %bitcast.8, bf16[3072,128]{1,0:T(8,128)(2,1)} %bitcast.9, f32[1,128]{1,0:T(1,128)} %bitcast.11, f32[1,128]{1,0:T(1,128)} %constant.2.clone.freq_ref, bf16[64,2048]{1,0:T(8,128)(2,1)} %bitcast.10), custom_call_target="tpu_custom_call" | custom-call | tf_op jit(solution)/shard_map/pallas_call | solution.py:305
  156.3 0.9 copy.9

commit v4 on v3

--- a/solution.py
+++ b/solution.py
@@ -13,7 +13,7 @@
 norm_eps = 1e-05
 MESH = pl.DeviceIdType.MESH
 f32, bf16 = jnp.float32, jnp.bfloat16
-EARLIER = (2, 4, 3, 2)
+EARLIER = (2, 4, 2, 2)
 LOW = len(EARLIER)
 CHUNK = 384
 

time: 157 us -> 157 us (level)
  the two profiles are of different devices: /device:TPU:32 before, /device:TPU:64 now
where the time goes in v4:
time: 157 us; the launch traced here: 156 us
  Pallas kernels  156 us (99%)
    pallas_call x1, Pallas kernels, on_device(): pl.pallas_call(functools.partial(kernel, n, cores, rows, cols), out_shape...  156 us

profile of v4, /device:TPU:64, one launch (start us, length us, event | category | flops | bytes accessed | tf_op | source)
XLA Modules:
  0.0 156.4 jit_solution(5052130513439321478)
XLA Ops:
  0.0 155.5 %shard_map.73 = bf16[192,2048]{1,0:T(8,128)(2,1)S(1)} custom-call(f32[16]{0:T(128)} %mix_ref.1, bf16[3072,128]{1,0:T(8,128)(2,1)} %bitcast.7, bf16[3072,128]{1,0:T(8,128)(2,1)} %bitcast.8, bf16[3072,128]{1,0:T(8,128)(2,1)} %bitcast.9, f32[1,128]{1,0:T(1,128)} %bitcast.11, f32[1,128]{1,0:T(1,128)} %constant.2.clone.freq_ref, bf16[64,2048]{1,0:T(8,128)(2,1)} %bitcast.10), custom_call_target="tpu_custom_call" | custom-call | tf_op jit(solution)/shard_map/pallas_call | solution.py:305
  155.5 0.9 copy.9
